TPU v7x, 256 devices: a whole 4x4x8 slice. The times are simulated.
256 devices in a mesh: sp: 32 (over z, x), tp: 4 (over y), dp: 2 (over core).
Axes of the slice: x: 4, y: 4, z: 8, core: 2. Of those that a mesh axis runs over, the one named last changes fastest.
Arguments:
- latents: bfloat16 [2, 8192, 4096], P('dp', ('sp', 'tp')), may hold values from -8 to 8
- cond: bfloat16 [2, 4096], P('dp', 'sp'), may hold values from -6 to 6
- cond_ctx: bfloat16 [4096], P('sp'), may hold values from -6 to 6
- context: bfloat16 [2, 1024, 4096], P('dp', 'sp'), may hold values from -8 to 8
- w_shift: bfloat16 [4096, 4096], P('sp', 'tp'), may hold values from -0.09375 to 0.09375
- w_scale: bfloat16 [4096, 4096], P('sp', 'tp'), may hold values from -0.09375 to 0.09375
- w_gate: bfloat16 [4096, 4096], P('sp', 'tp'), may hold values from -0.1875 to 0.1875
- gain_pre: bfloat16 [4096], replicated, may hold values from 0.099609375 to 1.8984375
- gain_post: bfloat16 [4096], replicated, may hold values from 0.099609375 to 1.8984375
- w_query: bfloat16 [4096, 1024], P('dp', 'tp'), may hold values from -0.09375 to 0.09375
- w_key: bfloat16 [4096, 1024], P('dp', 'tp'), may hold values from -0.09375 to 0.09375
- w_value: bfloat16 [4096, 2048], P('dp', 'tp'), may hold values from -0.09375 to 0.09375
- w_outgate: bfloat16 [4096, 2048], P('dp', 'tp'), may hold values from -0.09375 to 0.09375
- w_down: bfloat16 [4096, 32], replicated, may hold values from -0.25 to 0.25
- decay_up: bfloat16 [2, 16, 1024], P(None, None, 'tp'), may hold values from -1.5 to 1.5
- decay_bias: float32 [2, 1024], P(None, 'tp'), may hold values from -0.5 to 11
- head_gain: bfloat16 [2048], P('tp'), may hold values from 0.099609375 to 1.8984375
- w_out: bfloat16 [2048, 4096], P('tp', 'dp'), may hold values from -0.125 to 0.125
Outputs:
- mixer_out: bfloat16 [2, 8192, 4096], P('dp', ('sp', 'tp'))
All inputs are finite; a program needn't handle non-finite values.
Results may differ from a plain program's by a relative error of at most 0.015.
Values may be sent and summed in bfloat16 or wider, within the bound.
A program may use at most 128 MiB of HBM per device.

v0:
```python
import jax
import jax.numpy as jnp
from jax import lax
from jax.sharding import Mesh
from jax.sharding import PartitionSpec as P

DK_HEAD = 256
DV_HEAD = 512
RANK = 16
BLOCK = 128
SP_TP = ("sp_0", "sp_1", "tp")
SP = ("sp_0", "sp_1")
EPS = 1e-06
TAU = 16.0


def over_axes(value, axes):
    for axis in axes:
        value = lax.psum(value, axis)
    return value


def rows_first(arrays, axis, dims):
    turned = [jnp.moveaxis(a, dim, 0) for a, dim in zip(arrays, dims)]
    widths = [t[0].size for t in turned]
    both = jnp.concatenate([t.reshape(-1, w) for t, w in zip(turned, widths)], axis=1)
    result = lax.all_gather(both, axis, axis=0, tiled=True)
    tiles = jnp.split(result, [sum(widths[:k]) for k in range(1, len(widths))], axis=1)
    return tuple(
        (
            jnp.moveaxis(b.reshape(-1, *t.shape[1:]), 0, dim)
            for b, t, dim in zip(tiles, turned, dims)
        )
    )


def in_one_piece(arrays, axis, dim, along):
    ends, at = ([], 0)
    for a in arrays[:-1]:
        at += a.shape[along]
        ends.append(at)
    both = jnp.concatenate(arrays, axis=along)
    return tuple(jnp.split(lax.all_gather(both, axis, axis=dim, tiled=True), ends, axis=along))


def nothing_yet(value, identity):
    return jax.tree.map(
        lambda a, e: jnp.broadcast_to(jnp.asarray(e, a.dtype), a.shape), value, identity
    )


def prefix_by_axis(value, axes, combine, identity, reverse):
    before = start = nothing_yet(value, identity)
    total = value
    for axis in reversed(axes):
        count, mine = (lax.axis_size(axis), lax.axis_index(axis))
        pieces = jax.tree.map(lambda part: lax.all_gather(part, axis), total)
        inside, total = (start, start)
        for k in reversed(range(count)) if reverse else range(count):
            passed = k > mine if reverse else k < mine
            total = combine(total, jax.tree.map(lambda part: part[k], pieces))
            inside = jax.tree.map(lambda new, old: jnp.where(passed, new, old), total, inside)
        before = combine(inside, before)
    return before


def in_blocks(value, dim, count):
    lengths = value.shape
    tiles = value.reshape(*lengths[:dim], count, lengths[dim] // count, *lengths[dim + 1 :])
    return jnp.moveaxis(tiles, dim, 0)


def sent_and_summed(value, axis, dim):
    tiles = in_blocks(value, dim, lax.axis_size(axis))
    arrived = lax.all_to_all(tiles, axis, split_axis=0, concat_axis=0, tiled=True)
    return arrived.astype(jnp.float32).sum(axis=0)


def matmul(left, right):
    return jnp.dot(left, right, preferred_element_type=jnp.float32)


def rms_scale(vectors, gain):
    return vectors * lax.rsqrt(jnp.mean(vectors * vectors, axis=-1, keepdims=True) + EPS) * gain


def log_decays(lowrank, decay_up, decay_bias):
    result = []
    for direction in range(2):
        preact = (
            matmul(lowrank[:, direction * RANK : (direction + 1) * RANK], decay_up[direction])
            + decay_bias[direction]
        )
        result.append(jax.nn.log_sigmoid(preact) / TAU)
    return result


def chain(earlier, later):
    return (earlier[0] + later[0], earlier[1] * jnp.exp(later[0])[:, :, None] + later[1])


def reverse_rows(array):
    return jnp.flip(array, axis=1)


def local_pass(queries, keys_in, values, decays):
    heads_here, length, key_width = queries.shape
    count = length // BLOCK
    middle = BLOCK // 2

    def blocks(array):
        return jnp.moveaxis(array.reshape(heads_here, count, BLOCK, array.shape[-1]), 1, 0)

    causal = jnp.tril(jnp.ones((BLOCK, BLOCK), bool))

    def advance(carried_state, inputs):
        query_block_tile, key_block_tile, value_block_tile, block_g = inputs
        running_decay_sum = jnp.cumsum(block_g, axis=1)
        center = running_decay_sum[:, middle : middle + 1]
        scores = jnp.einsum(
            "htk,hsk->hts",
            query_block_tile * jnp.exp(running_decay_sum - center),
            key_block_tile * jnp.exp(center - running_decay_sum),
        )
        scores = jnp.where(causal, scores, 0.0)
        final_state_value = running_decay_sum[:, -1:]
        output = jnp.einsum("hts,hsv->htv", scores, value_block_tile) + jnp.einsum(
            "nyf,nfe->nye", query_block_tile * jnp.exp(running_decay_sum), carried_state
        )
        carried_state = carried_state * jnp.exp(final_state_value[:, 0])[:, :, None] + jnp.einsum(
            "dzg,dzu->dgu",
            key_block_tile * jnp.exp(final_state_value - running_decay_sum),
            value_block_tile,
        )
        return (carried_state, output)

    initial = jnp.zeros((heads_here, key_width, values.shape[-1]), jnp.float32)
    carried_state, output = lax.scan(
        advance, initial, (blocks(queries), blocks(keys_in), blocks(values), blocks(decays))
    )
    output = jnp.moveaxis(output, 0, 1).reshape(heads_here, length, values.shape[-1])
    return (output, carried_state, jnp.sum(decays, axis=1))


def body(
    latents,
    cond,
    cond_ctx,
    context,
    w_shift,
    w_scale,
    w_gate,
    gain_pre,
    gain_post,
    w_query,
    w_key,
    w_value,
    w_outgate,
    w_down,
    decay_up,
    decay_bias,
    head_gain,
    w_out,
):
    width = gain_pre.shape[0]
    column_count = w_shift.shape[1]
    column_start = lax.axis_index("tp") * column_count
    activated = jax.nn.silu(cond.astype(jnp.float32)).astype(jnp.bfloat16)
    activated_ctx = jax.nn.silu(cond_ctx.astype(jnp.float32)).astype(jnp.bfloat16)[None, :]

    def placed(part):
        return lax.dynamic_update_slice_in_dim(
            jnp.zeros((part.shape[0], width), jnp.float32), part, column_start, 1
        )

    shift_vec, scale_vec, gate_vec, shift_ctx, scale_ctx = (
        over_axes(placed(matmul(activated, w_shift)), SP_TP),
        over_axes(placed(matmul(activated, w_scale)), SP_TP),
        over_axes(placed(matmul(activated, w_gate)), SP_TP),
        over_axes(placed(matmul(activated_ctx, w_shift)), SP_TP),
        over_axes(placed(matmul(activated_ctx, w_scale)), SP_TP),
    )
    w_query, w_key, w_value, w_outgate, w_out = rows_first(
        (w_query, w_key, w_value, w_outgate, w_out), "dp", (0, 0, 0, 0, 1)
    )

    def project(rows, mats):
        return tuple((matmul(rows, weight).astype(jnp.bfloat16) for weight in mats))

    gain_in = gain_pre.astype(jnp.float32)
    latent_rows = latents[0].astype(jnp.float32)
    modulated = (rms_scale(latent_rows, gain_in) * (1.0 + scale_vec[0]) + shift_vec[0]).astype(
        jnp.bfloat16
    )
    lowrank = matmul(modulated, w_down).astype(jnp.bfloat16)
    all_rows, all_lowrank = in_one_piece((modulated, lowrank), "tp", 0, 1)
    queries, latent_keys, values, out_gate = project(all_rows, (w_query, w_key, w_value, w_outgate))
    decay_fwd, decay_bwd = log_decays(all_lowrank, decay_up, decay_bias)
    ctx_float = context[0].astype(jnp.float32)
    modulated_ctx = (rms_scale(ctx_float, gain_in) * (1.0 + scale_ctx[0]) + shift_ctx[0]).astype(
        jnp.bfloat16
    )
    keys_part, values_part = project(modulated_ctx, (w_key, w_value))
    ctx_keys, ctx_values, ctx_lowrank = in_one_piece(
        (keys_part, values_part, matmul(modulated_ctx, w_down).astype(jnp.bfloat16)), SP, 0, 1
    )
    heads_here = queries.shape[1] // DK_HEAD

    def by_head(array, head_width):
        return jnp.moveaxis(
            array.astype(jnp.float32).reshape(array.shape[0], heads_here, head_width), 1, 0
        )

    ctx_fwd, ctx_bwd = log_decays(ctx_lowrank, decay_up, decay_bias)
    ctx_head_keys = by_head(ctx_keys, DK_HEAD)
    ctx_head_values = by_head(ctx_values, DV_HEAD)
    ctx_head_fwd = by_head(ctx_fwd, DK_HEAD)
    ctx_head_bwd = by_head(ctx_bwd, DK_HEAD)
    ctx_cumulative = jnp.cumsum(ctx_head_fwd, axis=1)
    start_fwd = jnp.einsum(
        "dzg,dzu->dgu",
        ctx_head_keys * jnp.exp(ctx_cumulative[:, -1:] - ctx_cumulative),
        ctx_head_values,
    )
    start_bwd = jnp.einsum(
        "dzg,dzu->dgu",
        ctx_head_keys * jnp.exp(jnp.cumsum(ctx_head_bwd, axis=1) - ctx_head_bwd),
        ctx_head_values,
    )
    head_query_rows = by_head(queries, DK_HEAD) * DK_HEAD ** (-0.5)
    head_k = by_head(latent_keys, DK_HEAD)
    head_v = by_head(values, DV_HEAD)
    forward_head_output = by_head(decay_fwd, DK_HEAD)
    backward_head_output = reverse_rows(by_head(decay_bwd, DK_HEAD))
    out_fwd, state_fwd, total_fwd = local_pass(head_query_rows, head_k, head_v, forward_head_output)
    empty_pair = (jnp.zeros_like(total_fwd), jnp.zeros_like(state_fwd))
    prior_total, prior_state = prefix_by_axis((total_fwd, state_fwd), SP, chain, empty_pair, False)
    forward_entry_state = start_fwd * jnp.exp(prior_total)[:, :, None] + prior_state
    out_fwd = out_fwd + jnp.einsum(
        "nyf,nfe->nye",
        head_query_rows * jnp.exp(jnp.cumsum(forward_head_output, axis=1)),
        forward_entry_state,
    )
    reversed_query_rows = reverse_rows(head_query_rows)
    out_bwd, state_bwd, total_bwd = local_pass(
        reversed_query_rows, reverse_rows(head_k), reverse_rows(head_v), backward_head_output
    )
    later_total, later_state = prefix_by_axis((total_bwd, state_bwd), SP, chain, empty_pair, True)
    backward_entry_state = start_bwd * jnp.exp(later_total)[:, :, None] + later_state
    out_bwd = out_bwd + jnp.einsum(
        "nyf,nfe->nye",
        reversed_query_rows * jnp.exp(jnp.cumsum(backward_head_output, axis=1)),
        backward_entry_state,
    )
    mixed_sum = out_fwd + reverse_rows(out_bwd)
    gains_head = by_head(head_gain[None, :], DV_HEAD)
    gated_rows = rms_scale(mixed_sum, gains_head) * jax.nn.silu(by_head(out_gate, DV_HEAD))
    heads_out = (
        jnp.moveaxis(gated_rows, 0, 1)
        .reshape(gated_rows.shape[1], heads_here * DV_HEAD)
        .astype(jnp.bfloat16)
    )
    rounded = lax.optimization_barrier(matmul(heads_out, w_out).astype(jnp.bfloat16))
    projected = sent_and_summed(rounded.astype(jnp.float32).astype(jnp.bfloat16), "tp", 0)
    result_rows = latent_rows + gate_vec[0] * rms_scale(projected, gain_post.astype(jnp.float32))
    return result_rows.astype(jnp.bfloat16)[None]


def solution(mesh):
    finer = Mesh(
        mesh.devices.reshape(8, 4, mesh.shape["tp"], mesh.shape["dp"]), ("sp_0", "sp_1", "tp", "dp")
    )
    in_specs = (
        P("dp", SP_TP, None),
        P("dp", SP),
        P(SP),
        P("dp", SP, None),
        P(SP, "tp"),
        P(SP, "tp"),
        P(SP, "tp"),
        P(),
        P(),
        P("dp", "tp"),
        P("dp", "tp"),
        P("dp", "tp"),
        P("dp", "tp"),
        P(),
        P(None, None, "tp"),
        P(None, "tp"),
        P("tp"),
        P("tp", "dp"),
    )
    out_specs = P("dp", SP_TP, None)
    return jax.shard_map(body, mesh=finer, in_specs=in_specs, out_specs=out_specs, check_vma=False)
```

profile of v0, /device:TPU:2, one launch (start us, length us, event | category | flops | bytes accessed | tf_op | source)
XLA Modules:
  0.0 587.9 jit_solution(8418258431428282053)
XLA Ops:
  13.3 74.2 %all-reduce.7.cloned.1.call-done = (f32[1,4096]{1,0:T(1,128)}, f32[1,4096]{1,0:T(1,128)}, f32[1,4096]{1,0:T(1,128)}, f32[1,4096]{1,0:T(1,128)}, f32[1,4096]{1,0:T(1,128)}) async-done(((f32[1,4096]{1,0:T(1,128)}, f32[1,4096]{1,0:T(1,128)}, f32[1,4096]{1,0:T(1,128)}, f32[1,4096]{1,0:T(1,128)}, f32[1,4096]{1,0:T(1,128)}), (f32[1,4096]{1,0:T(1,128)}, f32[1,4096]{1,0:T(1,128)}, f32[1,4096]{1,0:T(1,128)}, ...) | async-done | bytes 81936 | tf_op jit(solution)/shard_map/psum | solution.py:19
  88.8 46.9 %all-reduce.11.cloned.1.call-done = (f32[1,4096]{1,0:T(1,128)}, f32[1,4096]{1,0:T(1,128)}, f32[1,4096]{1,0:T(1,128)}, f32[1,4096]{1,0:T(1,128)}, f32[1,4096]{1,0:T(1,128)}) async-done(((f32[1,4096]{1,0:T(1,128)}, f32[1,4096]{1,0:T(1,128)}, f32[1,4096]{1,0:T(1,128)}, f32[1,4096]{1,0:T(1,128)}, f32[1,4096]{1,0:T(1,128)}), (f32[1,4096]{1,0:T(1,128)}, f32[1,4096]{1,0:T(1,128)}, f32[1,4096]{1,0:T(1,128)}, ...) | async-done | bytes 81936 | tf_op jit(solution)/shard_map/psum | solution.py:19
  135.9 49.7 %all-reduce.9.cloned.1.call-done = (f32[4096]{0:T(1024)}, f32[1,4096]{1,0:T(1,128)}, f32[4096]{0:T(1024)}, f32[1,4096]{1,0:T(1,128)}, f32[4096]{0:T(1024)}) async-done(((f32[4096]{0:T(1024)}, f32[1,4096]{1,0:T(1,128)}, f32[4096]{0:T(1024)}, f32[1,4096]{1,0:T(1,128)}, f32[4096]{0:T(1024)}), (f32[4096]{0:T(1024)}, f32[1,4096]{1,0:T(1,128)}, f32[4096]{0:T(1024)}, f32[1,4096]{1,0:T(1,128)}, ...) | async-done | bytes 81936 | tf_op jit(solution)/shard_map/psum | solution.py:19
  210.1 13.2 %all-gather.14.cloned.1.call-done = bf16[256,4128]{1,0:T(8,128)(2,1)} async-done(((bf16[64,4128]{1,0:T(8,128)(2,1)}), bf16[256,4128]{1,0:T(8,128)(2,1)}) %all-gather.14.cloned.1.call-update) | async-done | bytes 2113552 | tf_op jit(solution)/shard_map/all_gather | solution.py:43
  224.7 35.7 %all-gather.16.cloned.1.call-done = bf16[4096,2048]{0,1:T(8,128)(2,1)} async-done(((bf16[2048,2048]{0,1:T(8,128)(2,1)}), bf16[4096,2048]{0,1:T(8,128)(2,1)}) %all-gather.16.cloned.1.call-update) | async-done | bytes 16777232 | tf_op jit(solution)/shard_map/all_gather | solution.py:27
  263.5 4.1 fusion.131
  268.0 3.0 broadcast_multiply_fusion.2
  272.7 3.5 while.27
  287.2 3.5 fusion.168
  291.4 8.0 %all-gather.5 = f32[4,1,256]{2,1,0:T(1,128)S(1)} all-gather(f32[1,1,256]{2,1,0:T(1,128)S(1)} %bitcast.746), channel_id=4, replica_groups=mesh['sp_0'=8,'sp_1'=4,'tp'=4,'dp'=2] {'sp_1'}, dimensions={0}, use_global_device_ids=true | all-gather | bytes 5120 | tf_op jit(solution)/shard_map/all_gather | solution.py:57
  299.5 11.4 %all-gather.26.cloned.1.call-done = f32[4,256,512]{2,1,0:T(8,128)} async-done(((f32[1,256,512]{2,1,0:T(8,128)}), f32[4,256,512]{2,1,0:T(8,128)}) %all-gather.26.cloned.1.call-update) | async-done | bytes 2097168 | tf_op jit(solution)/shard_map/all_gather | solution.py:57
  313.5 8.5 %all-gather.4 = f32[4,1,256]{2,1,0:T(1,128)S(1)} all-gather(f32[1,1,256]{2,1,0:T(1,128)S(1)} %bitcast.748), channel_id=2, replica_groups=mesh['sp_0'=8,'sp_1'=4,'tp'=4,'dp'=2] {'sp_1'}, dimensions={0}, use_global_device_ids=true | all-gather | bytes 5120 | tf_op jit(solution)/shard_map/all_gather | solution.py:57
  322.0 24.1 %all-gather.24.cloned.1.call-done = f32[4,256,512]{2,1,0:T(8,128)} async-done(((f32[1,256,512]{2,1,0:T(8,128)}), f32[4,256,512]{2,1,0:T(8,128)}) %all-gather.24.cloned.1.call-update) | async-done | bytes 2097168 | tf_op jit(solution)/shard_map/all_gather | solution.py:57
  349.5 16.6 %all_gather.60 = f32[8,1,256]{2,1,0:T(1,128)S(1)} all-gather(f32[1,1,256]{2,1,0:T(1,128)S(1)} %get-tuple-element.224), channel_id=1, replica_groups=mesh['sp_0'=8,'sp_1'=4,'tp'=4,'dp'=2] {'sp_0'}, dimensions={0}, use_global_device_ids=true | all-gather | bytes 9216 | tf_op jit(solution)/shard_map/all_gather | solution.py:57
  367.2 14.4 %all_gather.54 = f32[8,1,256]{2,1,0:T(1,128)S(1)} all-gather(f32[1,1,256]{2,1,0:T(1,128)S(1)} %get-tuple-element.220), channel_id=1, replica_groups=mesh['sp_0'=8,'sp_1'=4,'tp'=4,'dp'=2] {'sp_0'}, dimensions={0}, use_global_device_ids=true | all-gather | bytes 9216 | tf_op jit(solution)/shard_map/all_gather | solution.py:57
  384.5 41.4 %all-gather.18.cloned.1.call-done = bf16[1024,800]{1,0:T(8,128)(2,1)} async-done(((bf16[32,800]{1,0:T(8,128)(2,1)}), bf16[1024,800]{1,0:T(8,128)(2,1)}) %all-gather.18.cloned.1.call-update) | async-done | bytes 1638416 | tf_op jit(solution)/shard_map/all_gather | solution.py:43
  436.0 45.0 %all-gather.22.cloned.1.call-done = f32[8,1,256,512]{3,2,1,0:T(8,128)} async-done(((f32[1,1,256,512]{3,2,1,0:T(8,128)}), f32[8,1,256,512]{3,2,1,0:T(8,128)}) %all-gather.22.cloned.1.call-update) | async-done | bytes 4194320 | tf_op jit(solution)/shard_map/all_gather | solution.py:57
  481.1 6.1 %fusion.125 = f32[256,512]{1,0:T(8,128)} fusion(f32[256,512]{1,0:T(8,128)} %bitcast.715, f32[1,256,1024]{1,2,0:T(8,128)} %bitcast_add_fusion, f32[1024,256]{1,0:T(8,128)S(1)} %copy-done.11, bf16[1024,800]{1,0:T(8,128)(2,1)} %all-gather.18.cloned.1.call-done, f32[8,1,256,512]{3,2,1,0:T(8,128)} %all-gather.22.cloned.1.call-done, ...), kind=kOutput, calls=%fused_computation.130 | convolution fusion | flops 341573632 | bytes 11548684 | tf_op jit(solution)/shard_map/nyf,nfe->nye/dot_general | solution.py:250
  487.2 3.4 reverse.21
  490.6 45.4 %all-gather.20.cloned.1.call-done = f32[8,1,256,512]{3,2,1,0:T(8,128)} async-done(((f32[1,1,256,512]{3,2,1,0:T(8,128)}), f32[8,1,256,512]{3,2,1,0:T(8,128)}) %all-gather.20.cloned.1.call-update) | async-done | bytes 4194320 | tf_op jit(solution)/shard_map/all_gather | solution.py:57
  536.0 4.9 multiply_reduce_fusion.1
  541.0 8.0 %convolution_convert_fusion = bf16[256,4096]{1,0:T(8,128)(2,1)} fusion(bf16[4096,2048]{0,1:T(8,128)(2,1)} %all-gather.16.cloned.1.call-done, bf16[256,4128]{1,0:T(8,128)(2,1)} %all-gather.14.cloned.1.call-done, f32[256,512]{1,0:T(8,128)S(1)} %get-tuple-element.263, f32[512]{0:T(512)S(1)} %copy-done.36, f32[256]{0:T(256)S(1)} %add_rsqrt_fusion), kind=kOutput, calls=%fused_computation.90 | convolution fusion | flops 2149842944 | bytes 13110272 | tf_op jit(solution)/shard_map/dot_general | solution.py:80
  548.9 4.4 all-to-all-start
  553.4 26.2 %all-to-all-done = bf16[4,64,4096]{2,1,0:T(8,128)(2,1)S(1)} async-done(((bf16[4,64,4096]{2,1,0:T(8,128)(2,1)}), bf16[4,64,4096]{2,1,0:T(8,128)(2,1)S(1)}, u32[]{:S(2)}, u32[]{:S(2)}) %all-to-all-start) | async-done | bytes 2097184 | tf_op jit(solution)/shard_map/all_to_all | solution.py:75
  (240 shorter events, 77.6 us)
Async XLA Ops:
  6.5 179.7 %copy-start.5 = (bf16[1,64,4096]{2,1,0:T(8,128)(2,1)S(1)}, bf16[1,64,4096]{2,1,0:T(8,128)(2,1)}, u32[]{:S(2)}) copy-start(bf16[1,64,4096]{2,1,0:T(8,128)(2,1)} %param.22) | copy-start | bytes 1572868
  6.5 129.3 %copy-start.26 = (bf16[4096]{0:T(1024)(128)(2,1)S(1)}, bf16[4096]{0:T(1024)(128)(2,1)}, u32[]{:S(2)}) copy-start(bf16[4096]{0:T(1024)(128)(2,1)} %param.29) | copy-start | bytes 24580
  6.5 180.7 %copy-start.13 = (bf16[4096,32]{0,1:T(8,128)(2,1)S(1)}, bf16[4096,32]{0,1:T(8,128)(2,1)}, u32[]{:S(2)}) copy-start(bf16[4096,32]{0,1:T(8,128)(2,1)} %param.35) | copy-start | bytes 786436
  6.5 80.9 %all-reduce.7.cloned.1.call-start = ((), (), s32[]{:S(2)}) async-start(), calls=%async_computation.8 | async-start | bytes 163840 | tf_op jit(solution)/shard_map/psum | solution.py:19
  13.2 122.5 %all-reduce.11.cloned.1.call-start = ((), (), s32[]{:S(2)}) async-start(), calls=%async_computation.10 | async-start | bytes 163840 | tf_op jit(solution)/shard_map/psum | solution.py:19
  87.5 98.0 %all-reduce.9.cloned.1.call-start = ((), (), s32[]{:S(2)}) async-start(), calls=%async_computation.9 | async-start | bytes 163840 | tf_op jit(solution)/shard_map/psum | solution.py:19
  135.8 87.5 %all-gather.14.cloned.1.call-start = ((), (), s32[]{:S(2)}) async-start(), calls=%async_computation.1 | async-start | bytes 2703360 | tf_op jit(solution)/shard_map/all_gather | solution.py:43
  135.9 55.1 %copy-start.18 = (f32[4096]{0:T(1024)}, f32[4096]{0:T(1024)S(1)}, u32[]{:S(2)}) copy-start(f32[4096]{0:T(1024)S(1)} %convert_element_type.101) | copy-start | bytes 49156
  188.5 71.9 %all-gather.16.cloned.1.call-start = ((), (), s32[]{:S(2)}) async-start(), calls=%async_computation.2 | async-start | bytes 25165824 | tf_op jit(solution)/shard_map/all_gather | solution.py:27
  208.9 101.9 %all-gather.26.cloned.1.call-start = ((), (), s32[]{:S(2)}) async-start(), calls=%async_computation.7 | async-start | bytes 2621440 | tf_op jit(solution)/shard_map/all_gather | solution.py:57
  277.0 69.0 %all-gather.24.cloned.1.call-start = ((), (), s32[]{:S(2)}) async-start(), calls=%async_computation.6 | async-start | bytes 2621440 | tf_op jit(solution)/shard_map/all_gather | solution.py:57
  281.3 144.6 %all-gather.18.cloned.1.call-start = ((), (), s32[]{:S(2)}) async-start(), calls=%async_computation.3 | async-start | bytes 1892352 | tf_op jit(solution)/shard_map/all_gather | solution.py:43
  291.4 189.6 %all-gather.22.cloned.1.call-start = ((), (), s32[]{:S(2)}) async-start(), calls=%async_computation.5 | async-start | bytes 4718592 | tf_op jit(solution)/shard_map/all_gather | solution.py:57
  299.4 49.2 %copy-start.30 = (f32[1,1,256]{2,1,0:T(1,128)}, f32[1,1,256]{2,1,0:T(1,128)S(1)}, u32[]{:S(2)}) copy-start(f32[1,1,256]{2,1,0:T(1,128)S(1)} %get-tuple-element.253) | copy-start | bytes 3076
  299.4 49.1 %copy-start.32 = (f32[1,1,256]{2,1,0:T(1,128)}, f32[1,1,256]{2,1,0:T(1,128)S(1)}, u32[]{:S(2)}) copy-start(f32[1,1,256]{2,1,0:T(1,128)S(1)} %get-tuple-element.254) | copy-start | bytes 3076
  313.4 222.6 %all-gather.20.cloned.1.call-start = ((), (), s32[]{:S(2)}) async-start(), calls=%async_computation.4 | async-start | bytes 4718592 | tf_op jit(solution)/shard_map/all_gather | solution.py:57
  348.6 77.3 %copy-start.45 = (f32[1,256]{1,0:T(1,128)S(1)}, f32[1,256]{1,0:T(1,128)}, u32[]{:S(2)}) copy-start(f32[1,256]{1,0:T(1,128)} %copy-done.44) | copy-start | bytes 3076
  348.6 77.3 %copy-start.47 = (bf16[2,16,256]{2,1,0:T(8,128)(2,1)S(1)}, bf16[2,16,256]{2,1,0:T(8,128)(2,1)}, u32[]{:S(2)}) copy-start(bf16[2,16,256]{2,1,0:T(8,128)(2,1)} %param.36) | copy-start | bytes 49156
  481.0 55.0 %copy-start.9 = (f32[1,256,1024]{1,2,0:T(8,128)S(1)}, f32[1,256,1024]{1,2,0:T(8,128)}, u32[]{:S(2)}) copy-start(f32[1,256,1024]{1,2,0:T(8,128)} %copy-done.8) | copy-start | bytes 3145732
  481.0 55.0 %copy-start.16 = (f32[256,256]{1,0:T(8,128)S(1)}, f32[256,256]{1,0:T(8,128)}, u32[]{:S(2)}) copy-start(f32[256,256]{1,0:T(8,128)} %copy-done.15) | copy-start | bytes 786436
  481.1 55.0 %copy-start.17 = (f32[1,256,256]{1,2,0:T(8,128)S(1)}, f32[1,256,256]{1,2,0:T(8,128)}, u32[]{:S(2)}) copy-start(f32[1,256,256]{1,2,0:T(8,128)} %fusion.331) | copy-start | bytes 786436
  481.1 55.0 %copy-start.39 = (f32[1,1,256]{2,1,0:T(1,128)S(1)}, f32[1,1,256]{2,1,0:T(1,128)}, u32[]{:S(2)}) copy-start(f32[1,1,256]{2,1,0:T(1,128)} %get-tuple-element.218) | copy-start | bytes 3076
  481.1 55.0 %copy-start.41 = (f32[1,1,256]{2,1,0:T(1,128)S(1)}, f32[1,1,256]{2,1,0:T(1,128)}, u32[]{:S(2)}) copy-start(f32[1,1,256]{2,1,0:T(1,128)} %exp.528) | copy-start | bytes 3076
  548.9 30.6 %all-to-all-start = ((bf16[4,64,4096]{2,1,0:T(8,128)(2,1)}), bf16[4,64,4096]{2,1,0:T(8,128)(2,1)S(1)}, u32[]{:S(2)}, u32[]{:S(2)}) async-start(bf16[4,64,4096]{2,1,0:T(8,128)(2,1)} %bitcast.711), calls=%async_computation | async-start | bytes 4194304 | tf_op jit(solution)/shard_map/all_to_all | solution.py:75
  (37 other events, 557.8 us)
Sparse Core Ops, SparseCore 0:
  13.4 74.0 all-reduce.6
  90.2 45.5 all-reduce.10
  138.4 47.0 all-reduce.8
  188.6 34.5 all-gather.13
  224.9 35.4 all-gather.15
  277.1 33.6 all-gather.25
  312.7 33.3 all-gather.23
  348.6 77.2 all-gather.17
  427.7 53.2 all-gather.21
  482.6 53.3 all-gather.19
where the time goes:
time: 589 us; the launch traced here: 588 us
  waiting for transfers between devices  413 us (70%)
  matrix products  52.2 us (9%)
  blocking collectives  47.5 us (8%)
  local copies, waits for them, and re-layouts  34.5 us (6%)
  other arithmetic  21.2 us (4%)
  between operations  14.4 us (2%)
    psum x3, waiting for transfers between devices, over_axes(): value = lax.psum(value, axis)  171 us
    all_gather x4, waiting for transfers between devices, prefix_by_axis(): pieces = jax.tree.map(lambda part: lax.all_gather(part, axis), total)  126 us
    all_gather x2, waiting for transfers between devices, in_one_piece(): lax.all_gather(both, axis, axis=dim, tiled=True)  54.5 us
    all_gather x4, blocking collectives, prefix_by_axis(): pieces = jax.tree.map(lambda part: lax.all_gather(part, axis), total)  47.5 us
    dot_general x17, matrix products, matmul(): return jnp.dot(left, right, preferred_element_type=jnp.float32)  36.6 us
    all_gather x1, waiting for transfers between devices, rows_first(): result = lax.all_gather(both, axis, axis=0, tiled=True)  35.7 us
    all_to_all x1, waiting for transfers between devices, sent_and_summed(): lax.all_to_all(tiles, axis, split_axis=0, concat_axis=0, tiled=True)  26.2 us
    unnamed x108, local copies, waits for them, and re-layouts  24.2 us
  transfers between devices with their start and end apart: 11, of which 11 were waited for; matrix products, arithmetic and copies ran while one was open for 11% of the time, Pallas kernels for 0%

commit v1 on v0

--- a/solution.py
+++ b/solution.py
@@ -24,7 +24,10 @@
     turned = [jnp.moveaxis(a, dim, 0) for a, dim in zip(arrays, dims)]
     widths = [t[0].size for t in turned]
     both = jnp.concatenate([t.reshape(-1, w) for t, w in zip(turned, widths)], axis=1)
-    result = lax.all_gather(both, axis, axis=0, tiled=True)
+    count_2 = lax.axis_size(axis)
+    parts = jnp.stack([both for _ in range(count_2)])
+    parts = lax.all_to_all(parts, axis, split_axis=0, concat_axis=0)
+    result = jnp.concatenate(parts, axis=0)
     tiles = jnp.split(result, [sum(widths[:k]) for k in range(1, len(widths))], axis=1)
     return tuple(
         (

time: 589 us -> 554 us (0.941)
  waiting for transfers between devices: 413 us -> 380 us
  local copies, waits for them, and re-layouts: 34.5 us -> 20.4 us
  starting transfers between devices: 4.82 us -> 14.6 us
    all_gather x1 -> x0, waiting for transfers between devices: 35.7 us -> none  [rows_first(): result = lax.all_gather(both, axis, axis=0, tiled=True)]
    unnamed x108 -> x75, local copies, waits for them, and re-layouts: 24.2 us -> 12.4 us
    all_to_all x0 -> x1, starting transfers between devices: none -> 9.86 us  [rows_first(): parts = lax.all_to_all(parts, axis, split_axis=0, concat_axis=0)]
    another operation x10 -> x11, other arithmetic: 4.25 us -> 11 us  [the longest x1 6.76 us: rows_first(): parts = jnp.stack([both for _ in range(count_2)])]
  transfers between devices with their start and end apart: 11 -> 11, of which waited for: 11 -> 11; matrix products, arithmetic and copies ran while one was open for 11% -> 10% of each run, Pallas kernels for 0% -> 0%
where the time goes in v1:
time: 554 us; the launch traced here: 553 us
  waiting for transfers between devices  380 us (69%)
  matrix products  51.1 us (9%)
  blocking collectives  47.5 us (9%)
  other arithmetic  25.7 us (5%)
  local copies, waits for them, and re-layouts  20.4 us (4%)
  starting transfers between devices  14.6 us (3%)
  between operations  14 us (3%)
    psum x3, waiting for transfers between devices, over_axes(): value = lax.psum(value, axis)  171 us
    all_gather x4, waiting for transfers between devices, prefix_by_axis(): pieces = jax.tree.map(lambda part: lax.all_gather(part, axis), total)  126 us
    all_gather x2, waiting for transfers between devices, in_one_piece(): lax.all_gather(both, axis, axis=dim, tiled=True)  54.1 us
    all_gather x4, blocking collectives, prefix_by_axis(): pieces = jax.tree.map(lambda part: lax.all_gather(part, axis), total)  47.5 us
    dot_general x17, matrix products, matmul(): return jnp.dot(left, right, preferred_element_type=jnp.float32)  35.7 us
    all_to_all x1, waiting for transfers between devices, sent_and_summed(): lax.all_to_all(tiles, axis, split_axis=0, concat_axis=0, tiled=True)  26.2 us
    unnamed x75, local copies, waits for them, and re-layouts  12.4 us
  transfers between devices with their start and end apart: 11, of which 11 were waited for; matrix products, arithmetic and copies ran while one was open for 10% of the time, Pallas kernels for 0%

profile of v1, /device:TPU:2, one launch (start us, length us, event | category | flops | bytes accessed | tf_op | source)
XLA Modules:
  0.0 553.1 jit_solution(17573487321284094099)
XLA Ops:
  13.3 74.2 %all-reduce.7.cloned.1.call-done = (f32[1,4096]{1,0:T(1,128)}, f32[1,4096]{1,0:T(1,128)}, f32[1,4096]{1,0:T(1,128)}, f32[1,4096]{1,0:T(1,128)}, f32[1,4096]{1,0:T(1,128)}) async-done(((f32[1,4096]{1,0:T(1,128)}, f32[1,4096]{1,0:T(1,128)}, f32[1,4096]{1,0:T(1,128)}, f32[1,4096]{1,0:T(1,128)}, f32[1,4096]{1,0:T(1,128)}), (f32[1,4096]{1,0:T(1,128)}, f32[1,4096]{1,0:T(1,128)}, f32[1,4096]{1,0:T(1,128)}, ...) | async-done | bytes 81936 | tf_op jit(solution)/shard_map/psum | solution.py:19
  88.8 46.9 %all-reduce.11.cloned.1.call-done = (f32[1,4096]{1,0:T(1,128)}, f32[1,4096]{1,0:T(1,128)}, f32[1,4096]{1,0:T(1,128)}, f32[1,4096]{1,0:T(1,128)}, f32[1,4096]{1,0:T(1,128)}) async-done(((f32[1,4096]{1,0:T(1,128)}, f32[1,4096]{1,0:T(1,128)}, f32[1,4096]{1,0:T(1,128)}, f32[1,4096]{1,0:T(1,128)}, f32[1,4096]{1,0:T(1,128)}), (f32[1,4096]{1,0:T(1,128)}, f32[1,4096]{1,0:T(1,128)}, f32[1,4096]{1,0:T(1,128)}, ...) | async-done | bytes 81936 | tf_op jit(solution)/shard_map/psum | solution.py:19
  135.9 49.7 %all-reduce.9.cloned.1.call-done = (f32[4096]{0:T(1024)}, f32[1,4096]{1,0:T(1,128)}, f32[4096]{0:T(1024)}, f32[1,4096]{1,0:T(1,128)}, f32[4096]{0:T(1024)}) async-done(((f32[4096]{0:T(1024)}, f32[1,4096]{1,0:T(1,128)}, f32[4096]{0:T(1024)}, f32[1,4096]{1,0:T(1,128)}, f32[4096]{0:T(1024)}), (f32[4096]{0:T(1024)}, f32[1,4096]{1,0:T(1,128)}, f32[4096]{0:T(1024)}, f32[1,4096]{1,0:T(1,128)}, ...) | async-done | bytes 81936 | tf_op jit(solution)/shard_map/psum | solution.py:19
  196.6 6.8 %pad_maximum_fusion = bf16[2,2048,2048]{2,1,0:T(8,128)(2,1)} fusion(bf16[1,2048,2048]{2,1,0:T(8,128)(2,1)S(1)} %bitcast.703), kind=kLoop, calls=%fused_computation.90 | loop fusion | flops 8388608 | bytes 25165824 | tf_op jit(solution)/shard_map/stack | solution.py:28
  203.3 9.9 %all-to-all-start = ((bf16[2,2048,2048]{2,1,0:T(8,128)(2,1)}), bf16[2,2048,2048]{2,1,0:T(8,128)(2,1)}, u32[]{:S(2)}, u32[]{:S(2)}) async-start(bf16[2,2048,2048]{2,1,0:T(8,128)(2,1)} %pad_maximum_fusion), calls=%async_computation | async-start | bytes 33554432 | tf_op jit(solution)/shard_map/all_to_all | solution.py:29
  213.9 9.4 %all-gather.13.cloned.1.call-done = bf16[256,4128]{1,0:T(8,128)(2,1)} async-done(((bf16[64,4128]{1,0:T(8,128)(2,1)}), bf16[256,4128]{1,0:T(8,128)(2,1)}) %all-gather.13.cloned.1.call-update) | async-done | bytes 2113552 | tf_op jit(solution)/shard_map/all_gather | solution.py:46
  229.8 4.1 fusion.131
  238.8 3.5 while.27
  253.0 3.1 fusion.168
  256.8 8.0 %all-gather.5 = f32[4,1,256]{2,1,0:T(1,128)S(1)} all-gather(f32[1,1,256]{2,1,0:T(1,128)S(1)} %bitcast.749), channel_id=4, replica_groups=mesh['sp_0'=8,'sp_1'=4,'tp'=4,'dp'=2] {'sp_1'}, dimensions={0}, use_global_device_ids=true | all-gather | bytes 5120 | tf_op jit(solution)/shard_map/all_gather | solution.py:60
  264.8 11.7 %all-gather.23.cloned.1.call-done = f32[4,256,512]{2,1,0:T(8,128)} async-done(((f32[1,256,512]{2,1,0:T(8,128)}), f32[4,256,512]{2,1,0:T(8,128)}) %all-gather.23.cloned.1.call-update) | async-done | bytes 2097168 | tf_op jit(solution)/shard_map/all_gather | solution.py:60
  279.1 8.5 %all-gather.4 = f32[4,1,256]{2,1,0:T(1,128)S(1)} all-gather(f32[1,1,256]{2,1,0:T(1,128)S(1)} %bitcast.751), channel_id=2, replica_groups=mesh['sp_0'=8,'sp_1'=4,'tp'=4,'dp'=2] {'sp_1'}, dimensions={0}, use_global_device_ids=true | all-gather | bytes 5120 | tf_op jit(solution)/shard_map/all_gather | solution.py:60
  287.6 23.9 %all-gather.21.cloned.1.call-done = f32[4,256,512]{2,1,0:T(8,128)} async-done(((f32[1,256,512]{2,1,0:T(8,128)}), f32[4,256,512]{2,1,0:T(8,128)}) %all-gather.21.cloned.1.call-update) | async-done | bytes 2097168 | tf_op jit(solution)/shard_map/all_gather | solution.py:60
  314.4 16.6 %all_gather.56 = f32[8,1,256]{2,1,0:T(1,128)S(1)} all-gather(f32[1,1,256]{2,1,0:T(1,128)S(1)} %get-tuple-element.238), channel_id=1, replica_groups=mesh['sp_0'=8,'sp_1'=4,'tp'=4,'dp'=2] {'sp_0'}, dimensions={0}, use_global_device_ids=true | all-gather | bytes 9216 | tf_op jit(solution)/shard_map/all_gather | solution.py:60
  331.1 14.4 %all_gather.50 = f32[8,1,256]{2,1,0:T(1,128)S(1)} all-gather(f32[1,1,256]{2,1,0:T(1,128)S(1)} %get-tuple-element.234), channel_id=1, replica_groups=mesh['sp_0'=8,'sp_1'=4,'tp'=4,'dp'=2] {'sp_0'}, dimensions={0}, use_global_device_ids=true | all-gather | bytes 9216 | tf_op jit(solution)/shard_map/all_gather | solution.py:60
  346.7 44.7 %all-gather.15.cloned.1.call-done = bf16[1024,800]{1,0:T(8,128)(2,1)} async-done(((bf16[32,800]{1,0:T(8,128)(2,1)}), bf16[1024,800]{1,0:T(8,128)(2,1)}) %all-gather.15.cloned.1.call-update) | async-done | bytes 1638416 | tf_op jit(solution)/shard_map/all_gather | solution.py:46
  401.4 45.0 %all-gather.19.cloned.1.call-done = f32[8,1,256,512]{3,2,1,0:T(8,128)} async-done(((f32[1,1,256,512]{3,2,1,0:T(8,128)}), f32[8,1,256,512]{3,2,1,0:T(8,128)}) %all-gather.19.cloned.1.call-update) | async-done | bytes 4194320 | tf_op jit(solution)/shard_map/all_gather | solution.py:60
  446.5 6.0 %fusion.125 = f32[256,512]{1,0:T(8,128)} fusion(f32[256,512]{1,0:T(8,128)} %bitcast.718, f32[1,256,1024]{1,2,0:T(8,128)} %bitcast_add_fusion, f32[1024,256]{1,0:T(8,128)S(1)} %copy-done.10, bf16[1024,800]{1,0:T(8,128)(2,1)} %all-gather.15.cloned.1.call-done, f32[8,1,256,512]{3,2,1,0:T(8,128)} %all-gather.19.cloned.1.call-done, ...), kind=kOutput, calls=%fused_computation.131 | convolution fusion | flops 341573632 | bytes 11548684 | tf_op jit(solution)/shard_map/nyf,nfe->nye/dot_general | solution.py:253
  452.5 3.4 reverse.21
  456.0 45.7 %all-gather.17.cloned.1.call-done = f32[8,1,256,512]{3,2,1,0:T(8,128)} async-done(((f32[1,1,256,512]{3,2,1,0:T(8,128)}), f32[8,1,256,512]{3,2,1,0:T(8,128)}) %all-gather.17.cloned.1.call-update) | async-done | bytes 4194320 | tf_op jit(solution)/shard_map/all_gather | solution.py:60
  501.6 4.8 multiply_reduce_fusion.1
  506.5 7.9 %convolution_convert_fusion = bf16[256,4096]{1,0:T(8,128)(2,1)} fusion(bf16[4096,2048]{1,0:T(8,128)(2,1)} %bitcast.17, bf16[256,4128]{1,0:T(8,128)(2,1)} %all-gather.13.cloned.1.call-done, f32[256,512]{1,0:T(8,128)S(1)} %get-tuple-element.277, f32[512]{0:T(512)S(1)} %convert_element_type.118, f32[256]{0:T(256)S(1)} %add_rsqrt_fusion), kind=kOutput, calls=%fused_computation.91 | convolution fusion | flops 2149842944 | bytes 13110272 | tf_op jit(solution)/shard_map/dot_general | solution.py:83
  514.4 4.4 all-to-all-start.1
  518.8 26.2 %all-to-all-done.1 = bf16[4,64,4096]{2,1,0:T(8,128)(2,1)S(1)} async-done(((bf16[4,64,4096]{2,1,0:T(8,128)(2,1)}), bf16[4,64,4096]{2,1,0:T(8,128)(2,1)S(1)}, u32[]{:S(2)}, u32[]{:S(2)}) %all-to-all-start.1) | async-done | bytes 2097184 | tf_op jit(solution)/shard_map/all_to_all | solution.py:78
  (207 shorter events, 65.8 us)
Async XLA Ops:
  6.5 179.7 %copy-start.4 = (bf16[1,64,4096]{2,1,0:T(8,128)(2,1)S(1)}, bf16[1,64,4096]{2,1,0:T(8,128)(2,1)}, u32[]{:S(2)}) copy-start(bf16[1,64,4096]{2,1,0:T(8,128)(2,1)} %param.22) | copy-start | bytes 1572868
  6.5 129.3 %copy-start.24 = (bf16[4096]{0:T(1024)(128)(2,1)S(1)}, bf16[4096]{0:T(1024)(128)(2,1)}, u32[]{:S(2)}) copy-start(bf16[4096]{0:T(1024)(128)(2,1)} %param.29) | copy-start | bytes 24580
  6.5 180.7 %copy-start.12 = (bf16[4096,32]{0,1:T(8,128)(2,1)S(1)}, bf16[4096,32]{0,1:T(8,128)(2,1)}, u32[]{:S(2)}) copy-start(bf16[4096,32]{0,1:T(8,128)(2,1)} %param.35) | copy-start | bytes 786436
  6.5 80.9 %all-reduce.7.cloned.1.call-start = ((), (), s32[]{:S(2)}) async-start(), calls=%async_computation.8 | async-start | bytes 163840 | tf_op jit(solution)/shard_map/psum | solution.py:19
  13.2 122.5 %all-reduce.11.cloned.1.call-start = ((), (), s32[]{:S(2)}) async-start(), calls=%async_computation.10 | async-start | bytes 163840 | tf_op jit(solution)/shard_map/psum | solution.py:19
  87.5 98.0 %all-reduce.9.cloned.1.call-start = ((), (), s32[]{:S(2)}) async-start(), calls=%async_computation.9 | async-start | bytes 163840 | tf_op jit(solution)/shard_map/psum | solution.py:19
  135.8 87.5 %all-gather.13.cloned.1.call-start = ((), (), s32[]{:S(2)}) async-start(), calls=%async_computation.2 | async-start | bytes 2703360 | tf_op jit(solution)/shard_map/all_gather | solution.py:46
  135.8 55.5 %copy-start.16 = (f32[4096]{0:T(1024)}, f32[4096]{0:T(1024)S(1)}, u32[]{:S(2)}) copy-start(f32[4096]{0:T(1024)S(1)} %convert_element_type.101) | copy-start | bytes 49156
  203.3 9.9 %copy-start.26 = (f32[2,256]{1,0:T(2,128)S(1)}, f32[2,256]{1,0:T(2,128)}, u32[]{:S(2)}) copy-start(f32[2,256]{1,0:T(2,128)} %param.37) | copy-start | bytes 6148
  203.3 20.0 %copy-start.31 = (bf16[2,16,256]{2,1,0:T(8,128)(2,1)S(1)}, bf16[2,16,256]{2,1,0:T(8,128)(2,1)}, u32[]{:S(2)}) copy-start(bf16[2,16,256]{2,1,0:T(8,128)(2,1)} %param.36) | copy-start | bytes 49156
  203.3 23.4 %all-to-all-start = ((bf16[2,2048,2048]{2,1,0:T(8,128)(2,1)}), bf16[2,2048,2048]{2,1,0:T(8,128)(2,1)}, u32[]{:S(2)}, u32[]{:S(2)}) async-start(bf16[2,2048,2048]{2,1,0:T(8,128)(2,1)} %pad_maximum_fusion), calls=%async_computation | async-start | bytes 33554432 | tf_op jit(solution)/shard_map/all_to_all | solution.py:29
  213.2 63.3 %all-gather.23.cloned.1.call-start = ((), (), s32[]{:S(2)}) async-start(), calls=%async_computation.7 | async-start | bytes 2621440 | tf_op jit(solution)/shard_map/all_gather | solution.py:60
  243.2 68.4 %all-gather.21.cloned.1.call-start = ((), (), s32[]{:S(2)}) async-start(), calls=%async_computation.6 | async-start | bytes 2621440 | tf_op jit(solution)/shard_map/all_gather | solution.py:60
  247.5 143.9 %all-gather.15.cloned.1.call-start = ((), (), s32[]{:S(2)}) async-start(), calls=%async_computation.3 | async-start | bytes 1892352 | tf_op jit(solution)/shard_map/all_gather | solution.py:46
  256.8 189.7 %all-gather.19.cloned.1.call-start = ((), (), s32[]{:S(2)}) async-start(), calls=%async_computation.5 | async-start | bytes 4718592 | tf_op jit(solution)/shard_map/all_gather | solution.py:60
  279.0 35.1 %copy-start.27 = (bf16[512]{0:T(512)(128)(2,1)S(1)}, bf16[512]{0:T(512)(128)(2,1)}, u32[]{:S(2)}) copy-start(bf16[512]{0:T(512)(128)(2,1)} %param.38) | copy-start | bytes 3076
  279.0 222.6 %all-gather.17.cloned.1.call-start = ((), (), s32[]{:S(2)}) async-start(), calls=%async_computation.4 | async-start | bytes 4718592 | tf_op jit(solution)/shard_map/all_gather | solution.py:60
  314.1 77.3 %copy-start.30 = (f32[1,256]{1,0:T(1,128)S(1)}, f32[1,256]{1,0:T(1,128)}, u32[]{:S(2)}) copy-start(f32[1,256]{1,0:T(1,128)} %copy-done.29) | copy-start | bytes 3076
  314.1 77.3 %copy-start.32 = (bf16[2,16,256]{2,1,0:T(8,128)(2,1)S(1)}, bf16[2,16,256]{2,1,0:T(8,128)(2,1)}, u32[]{:S(2)}) copy-start(bf16[2,16,256]{2,1,0:T(8,128)(2,1)} %param.36) | copy-start | bytes 49156
  400.3 46.1 %copy-start.10 = (f32[1024,256]{1,0:T(8,128)S(1)}, f32[1024,256]{1,0:T(8,128)}, u32[]{:S(2)}) copy-start(f32[1024,256]{1,0:T(8,128)} %copy-done.9) | copy-start | bytes 3145732
  446.5 55.2 %copy-start.8 = (f32[1,256,1024]{1,2,0:T(8,128)S(1)}, f32[1,256,1024]{1,2,0:T(8,128)}, u32[]{:S(2)}) copy-start(f32[1,256,1024]{1,2,0:T(8,128)} %copy-done.7) | copy-start | bytes 3145732
  446.5 55.2 %copy-start.15 = (f32[256,256]{1,0:T(8,128)S(1)}, f32[256,256]{1,0:T(8,128)}, u32[]{:S(2)}) copy-start(f32[256,256]{1,0:T(8,128)} %copy-done.14) | copy-start | bytes 786436
  514.4 30.6 %all-to-all-start.1 = ((bf16[4,64,4096]{2,1,0:T(8,128)(2,1)}), bf16[4,64,4096]{2,1,0:T(8,128)(2,1)S(1)}, u32[]{:S(2)}, u32[]{:S(2)}) async-start(bf16[4,64,4096]{2,1,0:T(8,128)(2,1)} %bitcast.714), calls=%async_computation.1 | async-start | bytes 4194304 | tf_op jit(solution)/shard_map/all_to_all | solution.py:78
  518.8 26.7 %copy-start.23 = (f32[4096]{0:T(1024)S(1)}, f32[4096]{0:T(1024)}, u32[]{:S(2)}) copy-start(f32[4096]{0:T(1024)} %get-tuple-element.226) | copy-start | bytes 49156
  (22 other events, 63.7 us)
Sparse Core Ops, SparseCore 0:
  13.4 74.0 all-reduce.6
  90.1 45.5 all-reduce.10
  138.4 47.0 all-reduce.8
  188.6 34.5 all-gather.12
  243.3 33.1 all-gather.22
  278.1 33.3 all-gather.20
  314.1 77.2 all-gather.14
  393.2 53.2 all-gather.18
  448.3 53.3 all-gather.16
